TPU v7x, 256 devices: a whole 4x4x8 slice. The times are simulated.
256 devices in a mesh: sp: 16 (over y, x), tp: 16 (over z, core).
Axes of the slice: x: 4, y: 4, z: 8, core: 2. Of those that a mesh axis runs over, the one named last changes fastest.
Arguments:
- conv_value: bfloat16 [49152, 2048], P('sp', 'tp'), may hold values from -48 to 48
- conv_gate: bfloat16 [49152, 2048], P('sp', 'tp'), may hold values from -6 to 6
- doc_ids: int32 [49152], P('sp'), may hold values from 0 to 15, never falling along the last dimension, each value on 1 to 9216 neighbouring positions
- conv_kernel: bfloat16 [31, 2048], P(None, 'tp'), may hold values from -1 to 1
- norm_gain_conv: float32 [2048], replicated, may hold values from 0.1 to 1.9
- norm_bias_conv: float32 [2048], replicated, may hold values from -3 to 3
- proj_weight: bfloat16 [2048, 2048], P('tp'), may hold values from -0.125 to 0.125
- residual: bfloat16 [49152, 2048], P(('sp', 'tp')), may hold values from -6 to 6
- norm_gain_moe: float32 [2048], replicated, may hold values from 0.1 to 1.9
- group_router: bfloat16 [2048, 2], replicated, may hold values from -0.125 to 0.125
- expert_router: bfloat16 [2048, 16], replicated, may hold values from -0.125 to 0.125
- routing: int32 [49152, 2], P(('sp', 'tp')), may hold values from 0 to 15, as said below
- expert_gate_w: bfloat16 [16, 2048, 512], P('sp'), may hold values from -0.125 to 0.125
- expert_up_w: bfloat16 [16, 2048, 512], P('sp'), may hold values from -0.125 to 0.125
- expert_down_w: bfloat16 [16, 512, 2048], P('sp'), may hold values from -0.25 to 0.25
Outputs:
- output: bfloat16 [49152, 2048], P(('sp', 'tp'))
Inputs may be any that keep to these rules, and one draw needn't show every extreme that they name: `routing`: both numbers of a row are different experts of one group (expert // 8); within the rows of one device (aligned blocks of 192 rows) every expert is named exactly 24 times.
All inputs are finite; a program needn't handle non-finite values.
Results may differ from a plain program's by a relative error of at most 0.015.
Values may be sent and summed in bfloat16 or wider, within the bound.
No kernel may reach another device: no remote copies, remote signals or barrier semaphores. Data moves between devices by JAX's collectives and lax.ppermute only.
A program may use at most 64 MiB of HBM per device.

v0:
```python
import jax
import jax.numpy as jnp
from jax import lax
from jax.sharding import PartitionSpec as P

epsilon = 1e-06


def shifted(array, axis, by):
    count = lax.axis_size(axis)
    pairs = [(i, i + by) for i in range(count) if 0 <= i + by < count]
    return lax.ppermute(array, axis, pairs)


def project_rows(activated_rows, proj_weight):
    return jnp.dot(
        activated_rows,
        lax.all_gather(proj_weight, "tp", axis=0, tiled=True),
        preferred_element_type=jnp.float32,
    )


def body(
    conv_value,
    conv_gate,
    doc_ids,
    conv_kernel,
    norm_gain_conv,
    norm_bias_conv,
    proj_weight,
    residual,
    norm_gain_moe,
    group_router,
    expert_router,
    routing,
    expert_gate_w,
    expert_up_w,
    expert_down_w,
):
    local_tokens, local_width = conv_value.shape
    kernel_taps = conv_kernel.shape[0]
    rim_width = kernel_taps - 1
    gated_values = (
        conv_value.astype(jnp.float32) * jax.nn.sigmoid(conv_gate.astype(jnp.float32))
    ).astype(jnp.bfloat16)
    rim_values, rim_ids = shifted(
        (gated_values[local_tokens - rim_width :], doc_ids[local_tokens - rim_width :]), "sp", 1
    )
    padded = jnp.concatenate([rim_values, gated_values], axis=0)
    padded_ids = jnp.concatenate([rim_ids, doc_ids], axis=0)
    kernel = conv_kernel.astype(jnp.float32)
    summed = jnp.zeros((local_tokens, local_width), jnp.float32)
    for tap in range(kernel_taps):
        same_doc = padded_ids[tap : tap + local_tokens] == doc_ids
        summed = summed + jnp.where(
            same_doc[:, None],
            padded[tap : tap + local_tokens].astype(jnp.float32) * kernel[tap][None, :],
            jnp.float32(0.0),
        )
    convolved = summed.astype(jnp.bfloat16)
    raw_rows = lax.all_to_all(convolved, "tp", split_axis=0, concat_axis=1, tiled=True)
    raw_values = raw_rows.astype(jnp.float32)
    average = jnp.mean(raw_values, axis=1, keepdims=True)
    centered = raw_values - average
    variance = jnp.mean(centered * centered, axis=1, keepdims=True)
    moved_rows = jax.nn.silu(
        centered * lax.rsqrt(variance + epsilon) * norm_gain_conv + norm_bias_conv
    ).astype(jnp.bfloat16)
    projected = project_rows(moved_rows, proj_weight)
    state_values = residual.astype(jnp.float32) + projected
    hidden_state = state_values.astype(jnp.bfloat16)
    state_values = hidden_state.astype(jnp.float32)
    normed = (
        state_values
        * lax.rsqrt(jnp.mean(state_values * state_values, axis=1, keepdims=True) + epsilon)
        * norm_gain_moe
    ).astype(jnp.bfloat16)
    group_logits = jnp.dot(normed, group_router, preferred_element_type=jnp.float32)
    expert_logits = jnp.dot(normed, expert_router, preferred_element_type=jnp.float32)
    group_total = group_router.shape[1]
    expert_total = expert_router.shape[1]
    per_group = expert_total // group_total
    first_choice = routing[:, 0]
    second_choice = routing[:, 1]
    chosen_group = first_choice // per_group
    group_exp = jnp.exp(group_logits)
    group_match = chosen_group[:, None] == jnp.arange(group_total, dtype=jnp.int32)[None, :]
    group_prob = jnp.sum(jnp.where(group_match, group_exp, jnp.float32(0.0)), axis=1) / jnp.sum(
        group_exp, axis=1
    )
    expert_iota = jnp.arange(expert_total, dtype=jnp.int32)[None, :]
    first_logit = jnp.sum(
        jnp.where(first_choice[:, None] == expert_iota, expert_logits, jnp.float32(0.0)), axis=1
    )
    second_logit = jnp.sum(
        jnp.where(second_choice[:, None] == expert_iota, expert_logits, jnp.float32(0.0)), axis=1
    )
    first_exp = jnp.exp(first_logit)
    second_exp = jnp.exp(second_logit)
    first_weight = group_prob * first_exp / (first_exp + second_exp)
    second_weight = group_prob * second_exp / (first_exp + second_exp)
    row_count = normed.shape[0]
    capacity = 2 * row_count // expert_total
    flat_experts = routing.reshape(-1)
    indicator = (flat_experts[:, None] == expert_iota).astype(jnp.int32)
    before = jnp.cumsum(indicator, axis=0) - indicator
    position = jnp.sum(before * indicator, axis=1)
    destination = flat_experts * capacity + position
    source = (
        jnp.zeros((2 * row_count,), jnp.int32)
        .at[destination]
        .set(jnp.arange(2 * row_count, dtype=jnp.int32) // 2)
    )
    outgoing = normed[source].reshape(expert_total, capacity, normed.shape[1])
    arrived = lax.all_to_all(outgoing, "sp", split_axis=0, concat_axis=0, tiled=True)
    senders, slot_count, features = arrived.shape
    flattened = arrived.reshape(senders * slot_count, features)
    gate_part = jnp.dot(flattened, expert_gate_w[0], preferred_element_type=jnp.float32)
    up_part = jnp.dot(flattened, expert_up_w[0], preferred_element_type=jnp.float32)
    expert_hidden = (jax.nn.silu(gate_part) * up_part).astype(jnp.bfloat16)
    expert_result = jnp.dot(
        expert_hidden, expert_down_w[0], preferred_element_type=jnp.float32
    ).astype(jnp.bfloat16)
    returned = lax.all_to_all(
        expert_result.reshape(senders, slot_count, features),
        "sp",
        split_axis=0,
        concat_axis=0,
        tiled=True,
    )
    picked = (
        returned.reshape(2 * row_count, normed.shape[1])[destination]
        .reshape(row_count, 2, normed.shape[1])
        .astype(jnp.float32)
    )
    mixture = first_weight[:, None] * picked[:, 0] + second_weight[:, None] * picked[:, 1]
    return (state_values + mixture).astype(jnp.bfloat16)


def solution(mesh):
    placed = (
        P("sp", "tp"),
        P("sp", "tp"),
        P("sp"),
        P(None, "tp"),
        P(),
        P(),
        P("tp", None),
        P(("sp", "tp"), None),
        P(),
        P(),
        P(),
        P(("sp", "tp"), None),
        P("sp", None, None),
        P("sp", None, None),
        P("sp", None, None),
    )
    return jax.shard_map(
        body, mesh=mesh, in_specs=placed, out_specs=P(("sp", "tp"), None), check_vma=False
    )
```

profile of v0, /device:TPU:0, one launch (start us, length us, event | category | flops | bytes accessed | tf_op | source)
XLA Modules:
  0.0 186.5 jit_solution(3365401490658242660)
XLA Ops:
  6.5 0.7 all-gather.2.cloned.1.call-update
  7.3 0.8 slice.297
  8.0 1.7 collective-permute-start
  9.7 1.8 multiply_convert_fusion.2
  11.5 3.4 %collective-permute-start.1 = (bf16[30,128]{1,0:T(8,128)(2,1)S(1)}, bf16[30,128]{1,0:T(8,128)(2,1)S(1)}, u32[]{:S(2)}, u32[]{:S(2)}) collective-permute-start(bf16[30,128]{1,0:T(8,128)(2,1)S(1)} %slice.402), channel_id=1, source_target_pairs={{0,16},{16,32},{32,48},{48,64},{64,80},{80,96},{96,112},{112,128},... | collective-permute-start | bytes 23048 | tf_op jit(solution)/shard_map/ppermute | solution.py:12
  15.0 0.0 collective-permute-done
  15.0 0.0 copy-done.4
  15.0 0.1 fusion.72
  15.1 0.1 fusion.74
  15.2 0.1 fusion.76
  15.3 0.1 fusion.126
  15.4 0.8 collective-permute-done.1
  16.3 16.6 %add_convert_fusion = bf16[3072,128]{1,0:T(8,128)(2,1)} fusion(bf16[3072,128]{1,0:T(8,128)(2,1)S(1)} %multiply_convert_fusion.2, bf16[30,128]{1,0:T(8,128)(2,1)S(1)} %collective-permute-done.1, f32[128]{0:T(128)S(1)} %get-tuple-element.14, f32[128]{0:T(128)S(1)} %get-tuple-element.15, f32[128]{0:T(128)S(1)} %get-tuple-element.16, ...), kind=kLoop, calls=%fused_computation.60 | loop fusion | flops 83755008 | bytes 1688576 | tf_op jit(solution)/shard_map/convert_element_type | solution.py:60
  32.9 8.7 %all-to-all-start = ((bf16[16,192,128]{2,1,0:T(8,128)(2,1)}), bf16[16,192,128]{2,1,0:T(8,128)(2,1)S(1)}, u32[]{:S(2)}, u32[]{:S(2)}) async-start(bf16[16,192,128]{2,1,0:T(8,128)(2,1)} %bitcast.147), calls=%async_computation | async-start | bytes 1572864 | tf_op jit(solution)/shard_map/all_to_all | solution.py:61
  41.6 0.0 copy-done.6
  41.6 0.1 copy.25
  41.7 0.1 eq.206
  41.8 0.1 eq.202
  42.0 0.9 reduce-window.6
  42.9 0.2 slice_reduce_fusion
  43.1 0.1 copy.24
  43.3 0.1 mul.522
  43.4 0.1 fusion.67
  43.5 2.9 %scatter_custom_fusion = s32[384]{0:T(512)S(1)} fusion(s32[384]{0:T(512)S(1)} %fusion.132, s32[384]{0:T(512)S(1)} %add_select_fusion, s32[]{:T(128)} %constant.50.clone.1), kind=kCustom, calls=%fused_computation.261 | custom fusion | bytes 1540 | tf_op jit(solution)/shard_map/scatter | solution.py:112
  46.5 25.0 %all-to-all-done = bf16[16,192,128]{2,1,0:T(8,128)(2,1)S(1)} async-done(((bf16[16,192,128]{2,1,0:T(8,128)(2,1)}), bf16[16,192,128]{2,1,0:T(8,128)(2,1)S(1)}, u32[]{:S(2)}, u32[]{:S(2)}) %all-to-all-start) | async-done | bytes 786464 | tf_op jit(solution)/shard_map/all_to_all | solution.py:61
  71.5 0.2 convert_reduce_fusion
  71.7 0.4 fusion.8
  72.1 0.0 copy-start.7
  72.1 11.1 %all-gather.2.cloned.1.call-done = bf16[2048,2048]{1,0:T(8,128)(2,1)} async-done(((bf16[128,2048]{1,0:T(8,128)(2,1)}), bf16[2048,2048]{1,0:T(8,128)(2,1)}) %all-gather.2.cloned.1.call-update) | async-done | bytes 8388624 | tf_op jit(solution)/shard_map/all_gather | solution.py:18
  83.2 5.7 %multiply_reduce_fusion = (f32[192]{0:T(256)S(1)}, f32[192,2048]{1,0:T(8,128)S(1)}) fusion(bf16[2048,2048]{1,0:T(8,128)(2,1)} %all-gather.2.cloned.1.call-done, f32[2048]{0:T(1024)S(1)} %copy-done.11, f32[2048]{0:T(1024)S(1)} %copy-done.12, f32[192]{0:T(256)S(1)} %add_rsqrt_fusion.1, f32[192]{0:T(256)S(1)} %broadcast_multiply_fusion.1, ...), kind=kOutput, calls=%fused_computation.58 | convolution fusion | flops 1616903936 | bytes 11553024 | tf_op jit(solution)/shard_map/dot_general | solution.py:16
  88.9 0.0 copy-start.1
  88.9 1.1 copy-done.1
  90.0 0.2 multiply_convert_fusion
  90.2 3.1 %gather_fusion = bf16[384,2048]{1,0:T(8,128)(2,1)} fusion(bf16[192,2048]{1,0:T(8,128)(2,1)S(1)} %multiply_convert_fusion, s32[1024]{0:T(1024)S(1)} %pad_clamp_fusion.1), kind=kCustom, calls=%fused_computation | custom fusion | bytes 3147264 | tf_op jit(solution)/shard_map/gather | solution.py:114
  93.3 30.1 %all_to_all.23 = bf16[16,24,2048]{2,1,0:T(8,128)(2,1)S(1)} all-to-all(bf16[16,24,2048]{2,1,0:T(8,128)(2,1)} %bitcast.146), channel_id=1, replica_groups=mesh['sp'=16,'tp'=16] {'sp'}, dimensions={0} | all-to-all | bytes 3145728 | tf_op jit(solution)/shard_map/all_to_all | solution.py:115
  123.5 1.2 copy-done.3
  124.6 1.9 fusion.5
  126.5 0.0 copy-done
  126.5 5.3 %convolution_convert_fusion = bf16[384,2048]{1,0:T(8,128)(2,1)} fusion(bf16[1,512,2048]{2,1,0:T(8,128)(2,1)S(1)} %copy-done, bf16[384,2048]{1,0:T(8,128)(2,1)} %bitcast.150, bf16[1,2048,512]{2,1,0:T(8,128)(2,1)} %param.28, f32[384,512]{1,0:T(8,128)} %fusion.5), kind=kOutput, calls=%fused_computation.32 | convolution fusion | flops 1612578816 | bytes 8126464 | tf_op jit(solution)/shard_map/dot_general | solution.py:121
  131.8 4.7 %all-to-all-start.2 = ((bf16[16,24,2048]{2,1,0:T(8,128)(2,1)}), bf16[16,24,2048]{2,1,0:T(8,128)(2,1)}, u32[]{:S(2)}, u32[]{:S(2)}) async-start(bf16[16,24,2048]{2,1,0:T(8,128)(2,1)} %bitcast.148), calls=%async_computation.2 | async-start | bytes 3145728 | tf_op jit(solution)/shard_map/all_to_all | solution.py:124
  136.5 0.0 copy-done.8
  136.5 0.3 fusion.137
  136.9 0.3 select_reduce_fusion.1
  137.3 22.2 %all-to-all-done.2 = bf16[16,24,2048]{2,1,0:T(8,128)(2,1)} async-done(((bf16[16,24,2048]{2,1,0:T(8,128)(2,1)}), bf16[16,24,2048]{2,1,0:T(8,128)(2,1)}, u32[]{:S(2)}, u32[]{:S(2)}) %all-to-all-start.2) | async-done | bytes 1572896 | tf_op jit(solution)/shard_map/all_to_all | solution.py:124
  159.5 6.7 %gather_fusion.1 = bf16[384,2048]{1,0:T(8,128)(2,1)} fusion(bf16[384,2048]{1,0:T(8,128)(2,1)} %bitcast.43, s32[1024]{0:T(1024)S(1)} %pad_clamp_fusion), kind=kCustom, calls=%fused_computation.1 | custom fusion | bytes 3147264 | tf_op jit(solution)/shard_map/gather | solution.py:132
  166.2 4.7 %reshape.154 = f32[192,2,2048]{2,1,0:T(2,128)} reshape(bf16[384,2048]{1,0:T(8,128)(2,1)} %gather_fusion.1) | data formatting | bytes 4718592 | tf_op jit(solution)/shard_map/convert_element_type | solution.py:134
  170.9 6.2 %fusion.138 = (f32[192,1,2048]{2,1,0:T(1,128)S(1)}, f32[192,1,2048]{2,1,0:T(1,128)S(1)}) fusion(f32[192,2,2048]{2,1,0:T(2,128)} %reshape.154), kind=kLoop, calls=%fused_computation.302 | loop fusion | bytes 6291456 | tf_op jit(solution)/shard_map/slice | solution.py:136
  177.1 2.6 %fusion.15 = bf16[192,2048]{1,0:T(8,128)(2,1)} fusion(f32[192,2048]{1,0:T(8,128)S(1)} %copy-done.2, f32[192,1,2048]{2,1,0:T(1,128)S(1)} %get-tuple-element.12, f32[192,1,2048]{2,1,0:T(1,128)S(1)} %get-tuple-element.11, f32[192]{0:T(256)S(1)} %multiply_divide_fusion, f32[192]{0:T(256)S(1)} %get-tuple-element.9), kind=kLoop, calls=%fused_computation.54 | loop fusion | flops 1966080 | bytes 5506560 | tf_op jit(solution)/shard_map/convert_element_type | solution.py:137
  (37 shorter events, 0.2 us)
Async XLA Ops:
  6.5 119.9 %copy-start = (bf16[1,512,2048]{2,1,0:T(8,128)(2,1)S(1)}, bf16[1,512,2048]{2,1,0:T(8,128)(2,1)}, u32[]{:S(2)}) copy-start(bf16[1,512,2048]{2,1,0:T(8,128)(2,1)} %param.29) | copy-start | bytes 6291460
  6.5 8.5 %copy-start.4 = (s32[3072]{0:T(1024)S(1)}, s32[3072]{0:T(1024)}, u32[]{:S(2)}) copy-start(s32[3072]{0:T(1024)} %param.17) | copy-start | bytes 36868
  6.5 8.4 %copy-start.9 = (bf16[31,128]{1,0:T(8,128)(2,1)S(1)}, bf16[31,128]{1,0:T(8,128)(2,1)}, u32[]{:S(2)}) copy-start(bf16[31,128]{1,0:T(8,128)(2,1)} %param.18) | copy-start | bytes 23812
  6.5 76.6 %all-gather.2.cloned.1.call-start = ((), (), s32[]{:S(2)}) async-start(), calls=%async_computation.3 | async-start | bytes 8912896 | tf_op jit(solution)/shard_map/all_gather | solution.py:18
  8.0 7.0 %collective-permute-start = (s32[30]{0:T(128)S(1)}, s32[30]{0:T(128)S(1)}, u32[]{:S(2)}, u32[]{:S(2)}) collective-permute-start(s32[30]{0:T(128)S(1)} %slice.297), channel_id=1, source_target_pairs={{0,16},{16,32},{32,48},{48,64},{64,80},{80,96},{96,112},{112,128},... | collective-permute-start | bytes 368 | tf_op jit(solution)/shard_map/ppermute | solution.py:12
  11.5 4.8 %collective-permute-start.1 = (bf16[30,128]{1,0:T(8,128)(2,1)S(1)}, bf16[30,128]{1,0:T(8,128)(2,1)S(1)}, u32[]{:S(2)}, u32[]{:S(2)}) collective-permute-start(bf16[30,128]{1,0:T(8,128)(2,1)S(1)} %slice.402), channel_id=1, source_target_pairs={{0,16},{16,32},{32,48},{48,64},{64,80},{80,96},{96,112},{112,128},... | collective-permute-start | bytes 23048 | tf_op jit(solution)/shard_map/ppermute | solution.py:12
  16.3 25.3 %copy-start.6 = (s32[192,2]{0,1:T(2,128)S(1)}, s32[192,2]{0,1:T(2,128)}, u32[]{:S(2)}) copy-start(s32[192,2]{0,1:T(2,128)} %param.26) | copy-start | bytes 4612
  32.9 50.3 %copy-start.11 = (f32[2048]{0:T(1024)S(1)}, f32[2048]{0:T(1024)}, u32[]{:S(2)}) copy-start(f32[2048]{0:T(1024)} %param.20) | copy-start | bytes 24580
  32.9 50.3 %copy-start.12 = (f32[2048]{0:T(1024)S(1)}, f32[2048]{0:T(1024)}, u32[]{:S(2)}) copy-start(f32[2048]{0:T(1024)} %param.19) | copy-start | bytes 24580
  32.9 38.6 %all-to-all-start = ((bf16[16,192,128]{2,1,0:T(8,128)(2,1)}), bf16[16,192,128]{2,1,0:T(8,128)(2,1)S(1)}, u32[]{:S(2)}, u32[]{:S(2)}) async-start(bf16[16,192,128]{2,1,0:T(8,128)(2,1)} %bitcast.147), calls=%async_computation | async-start | bytes 1572864 | tf_op jit(solution)/shard_map/all_to_all | solution.py:61
  72.1 18.0 %copy-start.7 = (f32[2048]{0:T(1024)S(1)}, f32[2048]{0:T(1024)}, u32[]{:S(2)}) copy-start(f32[2048]{0:T(1024)} %param.23) | copy-start | bytes 24580
  88.9 1.1 copy-start.1
  93.3 31.3 %copy-start.10 = (bf16[1,2048,512]{2,1,0:T(8,128)(2,1)S(1)}, bf16[1,2048,512]{2,1,0:T(8,128)(2,1)}, u32[]{:S(2)}) copy-start(bf16[1,2048,512]{2,1,0:T(8,128)(2,1)} %param.27) | copy-start | bytes 6291460
  123.5 1.2 copy-start.3
  131.8 4.7 %copy-start.8 = (bf16[2048,2]{0,1:T(2,128)(2,1)S(1)}, bf16[2048,2]{0,1:T(2,128)(2,1)}, u32[]{:S(2)}) copy-start(bf16[2048,2]{0,1:T(2,128)(2,1)} %param.24) | copy-start | bytes 24580
  131.8 5.1 %copy-start.5 = (bf16[2048,16]{0,1:T(8,128)(2,1)S(1)}, bf16[2048,16]{0,1:T(8,128)(2,1)}, u32[]{:S(2)}) copy-start(bf16[2048,16]{0,1:T(8,128)(2,1)} %param.25) | copy-start | bytes 196612
  131.8 27.7 %all-to-all-start.2 = ((bf16[16,24,2048]{2,1,0:T(8,128)(2,1)}), bf16[16,24,2048]{2,1,0:T(8,128)(2,1)}, u32[]{:S(2)}, u32[]{:S(2)}) async-start(bf16[16,24,2048]{2,1,0:T(8,128)(2,1)} %bitcast.148), calls=%async_computation.2 | async-start | bytes 3145728 | tf_op jit(solution)/shard_map/all_to_all | solution.py:124
  170.9 6.2 %copy-start.2 = (f32[192,2048]{1,0:T(8,128)S(1)}, f32[192,2048]{1,0:T(8,128)}, u32[]{:S(2)}) copy-start(f32[192,2048]{1,0:T(8,128)} %copy-done.1) | copy-start | bytes 4718596
Sparse Core Ops, SparseCore 0:
  9.2 73.9 all-gather.1
where the time goes:
time: 187 us
  waiting for transfers between devices  59.9 us (32%)
  blocking collectives  30.1 us (16%)
  local copies, waits for them, and re-layouts  27.6 us (15%)
  other arithmetic  23.2 us (12%)
  starting transfers between devices  18.5 us (10%)
  between operations  13.7 us (7%)
  matrix products  13.5 us (7%)
    all_to_all x1, blocking collectives, body(): lax.all_to_all(outgoing, 'sp', split_axis=0, concat_axis=0, tiled=True)  30.1 us
    all_to_all x1, waiting for transfers between devices, body(): lax.all_to_all(convolved, 'tp', split_axis=0, concat_axis=1, tiled=True)  25 us
    all_to_all x1, waiting for transfers between devices, body(): lax.all_to_all(expert_result.reshape(senders, slot_count, features), 'sp'...  22.2 us
    convert_element_type x1, other arithmetic, body(): convolved = summed.astype(jnp.bfloat16)  16.6 us
    all_gather x1, waiting for transfers between devices, project_rows(): lax.all_gather(proj_weight, 'tp', axis=0, tiled=True)  11.1 us
    all_to_all x1, starting transfers between devices, body(): lax.all_to_all(convolved, 'tp', split_axis=0, concat_axis=1, tiled=True)  8.7 us
    gather x1, local copies, waits for them, and re-layouts, body(): returned.reshape(2 * row_count, normed.shape[1])[destination]  6.68 us
    slice x1, local copies, waits for them, and re-layouts, body(): picked[:, 0]  6.18 us
  transfers between devices with their start and end apart: 5, of which 4 were waited for; matrix products, arithmetic and copies ran while one was open for 14% of the time, Pallas kernels for 0%

commit v1 on v0

--- a/solution.py
+++ b/solution.py
@@ -1,9 +1,34 @@
+import functools
 import jax
 import jax.numpy as jnp
 from jax import lax
 from jax.sharding import PartitionSpec as P
 
 epsilon = 1e-06
+
+
+def group_quotas(mat, named_axis):
+    vec_out, low, local_next = (lax.psum(1, named_axis), lax.axis_index(named_axis), mat.shape[0])
+    fields = tuple(((it, (it + 1) % vec_out) for it in range(vec_out)))
+    windows = tuple(((it, (it - 1) % vec_out) for it in range(vec_out)))
+    reached = jnp.zeros((*mat.shape[:0], vec_out * local_next, *mat.shape[1:]), mat.dtype)
+    reached = lax.dynamic_update_slice_in_dim(reached, mat, low * local_next, axis=0)
+    frame_out = block_last = mat
+    aux = vec_out // 2
+    for i0 in range(1, aux + 1):
+        frame_out = lax.ppermute(frame_out, named_axis, fields)
+        reached = lax.dynamic_update_slice_in_dim(
+            reached, frame_out, (low - i0) % vec_out * local_next, axis=0
+        )
+        if i0 < vec_out - aux:
+            block_last = lax.ppermute(block_last, named_axis, windows)
+            reached = lax.dynamic_update_slice_in_dim(
+                reached, block_last, (low + i0) % vec_out * local_next, axis=0
+            )
+    return reached
+
+
+refer_steps_all_on = functools.partial(group_quotas, named_axis="tp")
 
 
 def shifted(array, axis, by):
@@ -14,9 +39,7 @@
 
 def project_rows(activated_rows, proj_weight):
     return jnp.dot(
-        activated_rows,
-        lax.all_gather(proj_weight, "tp", axis=0, tiled=True),
-        preferred_element_type=jnp.float32,
+        activated_rows, refer_steps_all_on(proj_weight), preferred_element_type=jnp.float32
     )
 
 

time: 187 us -> 226 us (1.21); the launches traced: 187 us -> 222 us
  local copies, waits for them, and re-layouts: 27.6 us -> 55 us
  starting transfers between devices: 18.5 us -> 39.3 us
  between operations: 13.7 us -> 0.33 us
  blocking collectives: 30.1 us -> 22.5 us
  other arithmetic: 23.2 us -> 29.7 us
  waiting for transfers between devices: 59.9 us -> 62.2 us
    ppermute x0 -> x15, waiting for transfers between devices: none -> 45.7 us  [the longest x8 41.7 us: group_quotas(): frame_out = lax.ppermute(frame_out, named_axis, fields)]
    all_to_all x1, waiting for transfers between devices: 25 us -> 0.01 us  [body(): lax.all_to_all(convolved, 'tp', split_axis=0, concat_axis=1, tiled=True)]
    ppermute x0 -> x15, starting transfers between devices: none -> 21.8 us  [the longest x7 21.3 us: group_quotas(): block_last = lax.ppermute(block_last, named_axis, windows)]
    dynamic_update_slice x0 -> x16, local copies, waits for them, and re-layouts: none -> 18.8 us  [the longest x8 11 us: group_quotas(): lax.dynamic_update_slice_in_dim(reached, frame_out, (low - i0) % vec_out...]
    all_gather x1 -> x0, waiting for transfers between devices: 11.1 us -> none  [project_rows(): lax.all_gather(proj_weight, 'tp', axis=0, tiled=True)]
    all_to_all x1, blocking collectives: 30.1 us -> 22.5 us  [body(): lax.all_to_all(outgoing, 'sp', split_axis=0, concat_axis=0, tiled=True)]
    all_to_all x1, waiting for transfers between devices: 22.2 us -> 16.5 us  [body(): lax.all_to_all(expert_result.reshape(senders, slot_count, features), 'sp'...]
    broadcast_in_dim x0 -> x1, local copies, waits for them, and re-layouts: none -> 4.28 us  [group_quotas(): jnp.zeros((*mat.shape[:0], vec_out * local_next, *mat.shape[1:]), mat.dtype)]
  transfers between devices with their start and end apart: 5 -> 19, of which waited for: 4 -> 12; matrix products, arithmetic and copies ran while one was open for 14% -> 26% of each run, Pallas kernels for 0% -> 0%
where the time goes in v1:
time: 226 us; the launch traced here: 222 us
  waiting for transfers between devices  62.2 us (28%)
  local copies, waits for them, and re-layouts  55 us (24%)
  starting transfers between devices  39.3 us (17%)
  other arithmetic  29.7 us (13%)
  blocking collectives  22.5 us (10%)
  matrix products  13.4 us (6%)
    ppermute x8, waiting for transfers between devices, group_quotas(): frame_out = lax.ppermute(frame_out, named_axis, fields)  41.7 us
    all_to_all x1, blocking collectives, body(): lax.all_to_all(outgoing, 'sp', split_axis=0, concat_axis=0, tiled=True)  22.5 us
    ppermute x7, starting transfers between devices, group_quotas(): block_last = lax.ppermute(block_last, named_axis, windows)  21.3 us
    all_to_all x1, waiting for transfers between devices, body(): lax.all_to_all(expert_result.reshape(senders, slot_count, features), 'sp'...  16.5 us
    convert_element_type x1, other arithmetic, body(): convolved = summed.astype(jnp.bfloat16)  16.4 us
    dynamic_update_slice x8, local copies, waits for them, and re-layouts, group_quotas(): lax.dynamic_update_slice_in_dim(reached, frame_out, (low - i0) % vec_out...  11 us
    dynamic_update_slice x7, local copies, waits for them, and re-layouts, group_quotas(): lax.dynamic_update_slice_in_dim(reached, block_last, (low + i0) % vec_out...  6.95 us
    ppermute x2, starting transfers between devices, shifted(): return lax.ppermute(array, axis, pairs)  6.78 us
  transfers between devices with their start and end apart: 19, of which 12 were waited for; matrix products, arithmetic and copies ran while one was open for 26% of the time, Pallas kernels for 0%

profile of v1, /device:TPU:0, one launch (start us, length us, event | category | flops | bytes accessed | tf_op | source)
XLA Modules:
  0.0 222.4 jit_solution(4869977696214443831)
XLA Ops:
  0.0 3.6 %collective-permute-start.3 = (bf16[128,2048]{1,0:T(8,128)(2,1)}, bf16[128,2048]{1,0:T(8,128)(2,1)S(1)}, u32[]{:S(2)}, u32[]{:S(2)}) collective-permute-start(bf16[128,2048]{1,0:T(8,128)(2,1)} %param.21), channel_id=1, source_target_pairs={{0,15},{1,0},{2,1},{3,2},{4,3},{5,4},{6,5},{7,6},{8,7},{9,8},{10,9... | collective-permute-start | bytes 1572872 | tf_op jit(solution)/shard_map/ppermute | solution.py:24
  3.7 1.3 slice.297
  4.9 3.9 %collective-permute-start = (s32[30]{0:T(128)}, s32[30]{0:T(128)}, u32[]{:S(2)}, u32[]{:S(2)}) collective-permute-start(s32[30]{0:T(128)} %slice.297), channel_id=1, source_target_pairs={{0,16},{16,32},{32,48},{48,64},{64,80},{80,96},{96,112},{112,128},... | collective-permute-start | bytes 368 | tf_op jit(solution)/shard_map/ppermute | solution.py:37
  8.9 1.8 multiply_convert_fusion.2
  11.3 2.8 %collective-permute-start.1 = (bf16[30,128]{1,0:T(8,128)(2,1)}, bf16[30,128]{1,0:T(8,128)(2,1)S(1)}, u32[]{:S(2)}, u32[]{:S(2)}) collective-permute-start(bf16[30,128]{1,0:T(8,128)(2,1)} %slice.402), channel_id=1, source_target_pairs={{0,16},{16,32},{32,48},{48,64},{64,80},{80,96},{96,112},{112,128},... | collective-permute-start | bytes 23048 | tf_op jit(solution)/shard_map/ppermute | solution.py:37
  22.2 3.1 %scatter_custom_fusion = s32[384]{0:T(512)S(1)} fusion(s32[384]{0:T(512)S(1)} %fusion.132, s32[384]{0:T(512)} %add_select_fusion, s32[]{:T(128)} %constant.138.clone.1), kind=kCustom, calls=%fused_computation.277 | custom fusion | bytes 2048 | tf_op jit(solution)/shard_map/scatter | solution.py:135
  25.3 1.1 fusion.72
  26.4 1.1 fusion.74
  27.5 1.1 fusion.76
  29.4 16.4 %add_convert_fusion = bf16[3072,128]{1,0:T(8,128)(2,1)} fusion(bf16[3072,128]{1,0:T(8,128)(2,1)S(1)} %multiply_convert_fusion.2, bf16[30,128]{1,0:T(8,128)(2,1)S(1)} %collective-permute-done.1, f32[128]{0:T(128)} %get-tuple-element.14, f32[128]{0:T(128)} %get-tuple-element.15, f32[128]{0:T(128)} %get-tuple-element.16, f32[128]{0:T(128)} %get-tuple-element.17, ...), kind=kLoop, calls=%fused_computation.60 | loop fusion | flops 83755008 | bytes 1688576 | tf_op jit(solution)/shard_map/convert_element_type | solution.py:83
  45.8 6.2 %all-to-all-start = ((bf16[16,192,128]{2,1,0:T(8,128)(2,1)}), bf16[16,192,128]{2,1,0:T(8,128)(2,1)S(1)}, u32[]{:S(2)}, u32[]{:S(2)}) async-start(bf16[16,192,128]{2,1,0:T(8,128)(2,1)} %bitcast.147), calls=%async_computation | async-start | bytes 1572864 | tf_op jit(solution)/shard_map/all_to_all | solution.py:84
  52.5 4.3 %broadcast_in_dim.280 = bf16[2048,2048]{1,0:T(8,128)(2,1)} broadcast(bf16[]{:T(256)} %constant.135.clone.1), dimensions={} | broadcast | bytes 8388610 | tf_op jit(solution)/shard_map/broadcast_in_dim | solution.py:14
  57.6 2.6 %collective-permute-start.5 = (bf16[128,2048]{1,0:T(8,128)(2,1)S(1)}, bf16[128,2048]{1,0:T(8,128)(2,1)}, u32[]{:S(2)}, u32[]{:S(2)}) collective-permute-start(bf16[128,2048]{1,0:T(8,128)(2,1)S(1)} %collective-permute-done.3), channel_id=1, source_target_pairs={{0,15},{1,0},{2,1},{3,2},{4,3},{5,4},{6,5},{7,6},{8,7},{9,8},{10,9... | collective-permute-start | bytes 1572872 | tf_op jit(solution)/shard_map/ppermute | solution.py:24
  60.2 18.7 %collective-permute-done.4 = bf16[128,2048]{1,0:T(8,128)(2,1)} collective-permute-done((bf16[128,2048]{1,0:T(8,128)(2,1)}, bf16[128,2048]{1,0:T(8,128)(2,1)}, u32[]{:S(2)}, u32[]{:S(2)}) %collective-permute-start.4) | collective-permute-done | bytes 524320 | tf_op jit(solution)/shard_map/ppermute | solution.py:19
  78.9 1.9 constant_dynamic-update-slice_fusion.14
  81.7 2.9 %collective-permute-start.7 = (bf16[128,2048]{1,0:T(8,128)(2,1)}, bf16[128,2048]{1,0:T(8,128)(2,1)S(1)}, u32[]{:S(2)}, u32[]{:S(2)}) collective-permute-start(bf16[128,2048]{1,0:T(8,128)(2,1)} %collective-permute-done.5), channel_id=1, source_target_pairs={{0,15},{1,0},{2,1},{3,2},{4,3},{5,4},{6,5},{7,6},{8,7},{9,8},{10,9... | collective-permute-start | bytes 1572872 | tf_op jit(solution)/shard_map/ppermute | solution.py:24
  84.6 1.9 constant_dynamic-update-slice_fusion.12
  86.5 2.6 %collective-permute-done.6 = bf16[128,2048]{1,0:T(8,128)(2,1)} collective-permute-done((bf16[128,2048]{1,0:T(8,128)(2,1)}, bf16[128,2048]{1,0:T(8,128)(2,1)}, u32[]{:S(2)}, u32[]{:S(2)}) %collective-permute-start.6) | collective-permute-done | bytes 524320 | tf_op jit(solution)/shard_map/ppermute | solution.py:19
  89.0 1.9 constant_dynamic-update-slice_fusion.11
  91.6 3.0 %collective-permute-start.9 = (bf16[128,2048]{1,0:T(8,128)(2,1)S(1)}, bf16[128,2048]{1,0:T(8,128)(2,1)S(1)}, u32[]{:S(2)}, u32[]{:S(2)}) collective-permute-start(bf16[128,2048]{1,0:T(8,128)(2,1)S(1)} %collective-permute-done.7), channel_id=1, source_target_pairs={{0,15},{1,0},{2,1},{3,2},{4,3},{5,4},{6,5},{7,6},{8,7},{9,8},{10,9... | collective-permute-start | bytes 1572872 | tf_op jit(solution)/shard_map/ppermute | solution.py:24
  94.6 4.6 %collective-permute-done.8 = bf16[128,2048]{1,0:T(8,128)(2,1)} collective-permute-done((bf16[128,2048]{1,0:T(8,128)(2,1)}, bf16[128,2048]{1,0:T(8,128)(2,1)}, u32[]{:S(2)}, u32[]{:S(2)}) %collective-permute-start.8) | collective-permute-done | bytes 524320 | tf_op jit(solution)/shard_map/ppermute | solution.py:19
  99.5 1.8 collective-permute-done.9
  101.3 3.1 %collective-permute-start.11 = (bf16[128,2048]{1,0:T(8,128)(2,1)S(1)}, bf16[128,2048]{1,0:T(8,128)(2,1)S(1)}, u32[]{:S(2)}, u32[]{:S(2)}) collective-permute-start(bf16[128,2048]{1,0:T(8,128)(2,1)S(1)} %collective-permute-done.9), channel_id=1, source_target_pairs={{0,15},{1,0},{2,1},{3,2},{4,3},{5,4},{6,5},{7,6},{8,7},{9,8},{10,9... | collective-permute-start | bytes 1572872 | tf_op jit(solution)/shard_map/ppermute | solution.py:24
  104.4 1.9 constant_dynamic-update-slice_fusion.10
  106.3 2.9 %collective-permute-done.10 = bf16[128,2048]{1,0:T(8,128)(2,1)S(1)} collective-permute-done((bf16[128,2048]{1,0:T(8,128)(2,1)}, bf16[128,2048]{1,0:T(8,128)(2,1)S(1)}, u32[]{:S(2)}, u32[]{:S(2)}) %collective-permute-start.10) | collective-permute-done | bytes 524320 | tf_op jit(solution)/shard_map/ppermute | solution.py:19
  110.0 1.9 constant_dynamic-update-slice_fusion.8
  111.9 3.0 %collective-permute-start.13 = (bf16[128,2048]{1,0:T(8,128)(2,1)S(1)}, bf16[128,2048]{1,0:T(8,128)(2,1)S(1)}, u32[]{:S(2)}, u32[]{:S(2)}) collective-permute-start(bf16[128,2048]{1,0:T(8,128)(2,1)S(1)} %collective-permute-done.11), channel_id=1, source_target_pairs={{0,15},{1,0},{2,1},{3,2},{4,3},{5,4},{6,5},{7,6},{8,7},{9,8},{10,9... | collective-permute-start | bytes 1572872 | tf_op jit(solution)/shard_map/ppermute | solution.py:24
  114.9 0.9 constant_dynamic-update-slice_fusion.7
  115.7 3.3 %collective-permute-done.12 = bf16[128,2048]{1,0:T(8,128)(2,1)S(1)} collective-permute-done((bf16[128,2048]{1,0:T(8,128)(2,1)S(1)}, bf16[128,2048]{1,0:T(8,128)(2,1)S(1)}, u32[]{:S(2)}, u32[]{:S(2)}) %collective-permute-start.12) | collective-permute-done | bytes 524320 | tf_op jit(solution)/shard_map/ppermute | solution.py:19
  120.7 0.9 collective-permute-done.13
  121.6 3.1 %collective-permute-start.15 = (bf16[128,2048]{1,0:T(8,128)(2,1)S(1)}, bf16[128,2048]{1,0:T(8,128)(2,1)S(1)}, u32[]{:S(2)}, u32[]{:S(2)}) collective-permute-start(bf16[128,2048]{1,0:T(8,128)(2,1)S(1)} %collective-permute-done.13), channel_id=1, source_target_pairs={{0,15},{1,0},{2,1},{3,2},{4,3},{5,4},{6,5},{7,6},{8,7},{9,8},{10,9... | collective-permute-start | bytes 1572872 | tf_op jit(solution)/shard_map/ppermute | solution.py:24
  124.7 0.9 constant_dynamic-update-slice_fusion.4
  125.6 3.2 %collective-permute-done.14 = bf16[128,2048]{1,0:T(8,128)(2,1)S(1)} collective-permute-done((bf16[128,2048]{1,0:T(8,128)(2,1)S(1)}, bf16[128,2048]{1,0:T(8,128)(2,1)S(1)}, u32[]{:S(2)}, u32[]{:S(2)}) %collective-permute-start.14) | collective-permute-done | bytes 524320 | tf_op jit(solution)/shard_map/ppermute | solution.py:19
  130.5 0.9 collective-permute-done.15
  132.2 6.4 %collective-permute-done.16 = bf16[128,2048]{1,0:T(8,128)(2,1)S(1)} collective-permute-done((bf16[128,2048]{1,0:T(8,128)(2,1)S(1)}, bf16[128,2048]{1,0:T(8,128)(2,1)S(1)}, u32[]{:S(2)}, u32[]{:S(2)}) %collective-permute-start.16) | collective-permute-done | bytes 524320 | tf_op jit(solution)/shard_map/ppermute | solution.py:19
  139.5 5.6 %multiply_reduce_fusion = (f32[192]{0:T(256)S(1)}, f32[192,2048]{1,0:T(8,128)S(1)}) fusion(bf16[2048,2048]{1,0:T(8,128)(2,1)} %constant_dynamic-update-slice_fusion, f32[2048]{0:T(1024)S(1)} %copy-done.15, f32[2048]{0:T(1024)S(1)} %copy-done.16, f32[192]{0:T(256)S(1)} %add_rsqrt_fusion.1, f32[192]{0:T(256)S(1)} %broadcast_multiply_fusion.1, ...), kind=kOutput, calls=%fused_computation.58 | convolution fusion | flops 1616903936 | bytes 11553024 | tf_op jit(solution)/shard_map/dot_general | solution.py:41
  145.1 1.1 copy-done.1
  146.4 3.1 %gather_fusion = bf16[384,2048]{1,0:T(8,128)(2,1)} fusion(bf16[192,2048]{1,0:T(8,128)(2,1)S(1)} %multiply_convert_fusion, s32[1024]{0:T(1024)S(1)} %pad_clamp_fusion.1), kind=kCustom, calls=%fused_computation | custom fusion | bytes 3147264 | tf_op jit(solution)/shard_map/gather | solution.py:137
  149.6 22.5 %all_to_all.23 = bf16[16,24,2048]{2,1,0:T(8,128)(2,1)S(1)} all-to-all(bf16[16,24,2048]{2,1,0:T(8,128)(2,1)} %bitcast.146), channel_id=1, replica_groups=mesh['sp'=16,'tp'=16] {'sp'}, dimensions={0} | all-to-all | bytes 3145728 | tf_op jit(solution)/shard_map/all_to_all | solution.py:138
  172.0 1.2 copy-done.3
  173.2 1.9 fusion.5
  175.1 5.3 %convolution_convert_fusion = bf16[384,2048]{1,0:T(8,128)(2,1)} fusion(bf16[1,512,2048]{2,1,0:T(8,128)(2,1)S(1)} %copy-done, bf16[384,2048]{1,0:T(8,128)(2,1)} %bitcast.150, bf16[1,2048,512]{2,1,0:T(8,128)(2,1)} %param.28, f32[384,512]{1,0:T(8,128)} %fusion.5), kind=kOutput, calls=%fused_computation.32 | convolution fusion | flops 1612578816 | bytes 8126464 | tf_op jit(solution)/shard_map/dot_general | solution.py:144
  180.4 4.5 %all-to-all-start.2 = ((bf16[16,24,2048]{2,1,0:T(8,128)(2,1)}), bf16[16,24,2048]{2,1,0:T(8,128)(2,1)}, u32[]{:S(2)}, u32[]{:S(2)}) async-start(bf16[16,24,2048]{2,1,0:T(8,128)(2,1)} %bitcast.148), calls=%async_computation.2 | async-start | bytes 3145728 | tf_op jit(solution)/shard_map/all_to_all | solution.py:147
  185.7 16.5 %all-to-all-done.2 = bf16[16,24,2048]{2,1,0:T(8,128)(2,1)} async-done(((bf16[16,24,2048]{2,1,0:T(8,128)(2,1)}), bf16[16,24,2048]{2,1,0:T(8,128)(2,1)}, u32[]{:S(2)}, u32[]{:S(2)}) %all-to-all-start.2) | async-done | bytes 1572896 | tf_op jit(solution)/shard_map/all_to_all | solution.py:147
  202.2 6.7 %gather_fusion.1 = bf16[384,2048]{1,0:T(8,128)(2,1)} fusion(bf16[384,2048]{1,0:T(8,128)(2,1)} %bitcast.43, s32[1024]{0:T(1024)S(1)} %pad_clamp_fusion), kind=kCustom, calls=%fused_computation.1 | custom fusion | bytes 3147264 | tf_op jit(solution)/shard_map/gather | solution.py:155
  208.9 4.7 %reshape.154 = f32[192,2,2048]{2,1,0:T(2,128)} reshape(bf16[384,2048]{1,0:T(8,128)(2,1)} %gather_fusion.1) | data formatting | bytes 4718592 | tf_op jit(solution)/shard_map/convert_element_type | solution.py:157
  213.6 6.2 %fusion.138 = (f32[192,1,2048]{2,1,0:T(1,128)S(1)}, f32[192,1,2048]{2,1,0:T(1,128)S(1)}) fusion(f32[192,2,2048]{2,1,0:T(2,128)} %reshape.154), kind=kLoop, calls=%fused_computation.318 | loop fusion | bytes 6291456 | tf_op jit(solution)/shard_map/slice | solution.py:159
  219.8 2.6 %fusion.15 = bf16[192,2048]{1,0:T(8,128)(2,1)} fusion(f32[192,2048]{1,0:T(8,128)S(1)} %copy-done.2, f32[192,1,2048]{2,1,0:T(1,128)S(1)} %get-tuple-element.12, f32[192,1,2048]{2,1,0:T(1,128)S(1)} %get-tuple-element.11, f32[192]{0:T(256)S(1)} %multiply_divide_fusion, f32[192]{0:T(256)S(1)} %get-tuple-element.9), kind=kLoop, calls=%fused_computation.54 | loop fusion | flops 1966080 | bytes 5506560 | tf_op jit(solution)/shard_map/convert_element_type | solution.py:160
  (89 shorter events, 19.4 us)
Async XLA Ops:
  0.0 175.1 %copy-start = (bf16[1,512,2048]{2,1,0:T(8,128)(2,1)S(1)}, bf16[1,512,2048]{2,1,0:T(8,128)(2,1)}, u32[]{:S(2)}) copy-start(bf16[1,512,2048]{2,1,0:T(8,128)(2,1)} %param.29) | copy-start | bytes 6291460
  0.0 25.3 %copy-start.5 = (s32[3072]{0:T(1024)S(1)}, s32[3072]{0:T(1024)}, u32[]{:S(2)}) copy-start(s32[3072]{0:T(1024)} %param.17) | copy-start | bytes 36868
  0.0 14.1 %copy-start.10 = (bf16[31,128]{1,0:T(8,128)(2,1)S(1)}, bf16[31,128]{1,0:T(8,128)(2,1)}, u32[]{:S(2)}) copy-start(bf16[31,128]{1,0:T(8,128)(2,1)} %param.18) | copy-start | bytes 23812
  0.0 15.4 %copy-start.7 = (s32[192,2]{0,1:T(2,128)S(1)}, s32[192,2]{0,1:T(2,128)}, u32[]{:S(2)}) copy-start(s32[192,2]{0,1:T(2,128)} %param.26) | copy-start | bytes 4612
  0.0 52.0 %collective-permute-start.2 = (bf16[128,2048]{1,0:T(8,128)(2,1)}, bf16[128,2048]{1,0:T(8,128)(2,1)}, u32[]{:S(2)}, u32[]{:S(2)}) collective-permute-start(bf16[128,2048]{1,0:T(8,128)(2,1)} %param.21), channel_id=1, source_target_pairs={{0,1},{1,2},{2,3},{3,4},{4,5},{5,6},{6,7},{7,8},{8,9},{9,10},{10,1... | collective-permute-start | bytes 1572872 | tf_op jit(solution)/shard_map/ppermute | solution.py:19
  0.0 57.5 %collective-permute-start.3 = (bf16[128,2048]{1,0:T(8,128)(2,1)}, bf16[128,2048]{1,0:T(8,128)(2,1)S(1)}, u32[]{:S(2)}, u32[]{:S(2)}) collective-permute-start(bf16[128,2048]{1,0:T(8,128)(2,1)} %param.21), channel_id=1, source_target_pairs={{0,15},{1,0},{2,1},{3,2},{4,3},{5,4},{6,5},{7,6},{8,7},{9,8},{10,9... | collective-permute-start | bytes 1572872 | tf_op jit(solution)/shard_map/ppermute | solution.py:24
  4.9 20.3 %collective-permute-start = (s32[30]{0:T(128)}, s32[30]{0:T(128)}, u32[]{:S(2)}, u32[]{:S(2)}) collective-permute-start(s32[30]{0:T(128)} %slice.297), channel_id=1, source_target_pairs={{0,16},{16,32},{32,48},{48,64},{64,80},{80,96},{96,112},{112,128},... | collective-permute-start | bytes 368 | tf_op jit(solution)/shard_map/ppermute | solution.py:37
  11.3 18.2 %collective-permute-start.1 = (bf16[30,128]{1,0:T(8,128)(2,1)}, bf16[30,128]{1,0:T(8,128)(2,1)S(1)}, u32[]{:S(2)}, u32[]{:S(2)}) collective-permute-start(bf16[30,128]{1,0:T(8,128)(2,1)} %slice.402), channel_id=1, source_target_pairs={{0,16},{16,32},{32,48},{48,64},{64,80},{80,96},{96,112},{112,128},... | collective-permute-start | bytes 23048 | tf_op jit(solution)/shard_map/ppermute | solution.py:37
  22.2 3.1 %copy-start.11 = (s32[384]{0:T(512)}, s32[384]{0:T(512)S(1)}, u32[]{:S(2)}) copy-start(s32[384]{0:T(512)S(1)} %fusion.132) | copy-start | bytes 4612
  45.8 45.1 %all-to-all-start = ((bf16[16,192,128]{2,1,0:T(8,128)(2,1)}), bf16[16,192,128]{2,1,0:T(8,128)(2,1)S(1)}, u32[]{:S(2)}, u32[]{:S(2)}) async-start(bf16[16,192,128]{2,1,0:T(8,128)(2,1)} %bitcast.147), calls=%async_computation | async-start | bytes 1572864 | tf_op jit(solution)/shard_map/all_to_all | solution.py:84
  52.0 26.9 %collective-permute-start.4 = (bf16[128,2048]{1,0:T(8,128)(2,1)}, bf16[128,2048]{1,0:T(8,128)(2,1)}, u32[]{:S(2)}, u32[]{:S(2)}) collective-permute-start(bf16[128,2048]{1,0:T(8,128)(2,1)} %collective-permute-done.2), channel_id=1, source_target_pairs={{0,1},{1,2},{2,3},{3,4},{4,5},{5,6},{6,7},{7,8},{8,9},{9,10},{10,1... | collective-permute-start | bytes 1572872 | tf_op jit(solution)/shard_map/ppermute | solution.py:19
  52.4 4.3 %copy-start.4 = (bf16[128,2048]{1,0:T(8,128)(2,1)S(1)}, bf16[128,2048]{1,0:T(8,128)(2,1)}, u32[]{:S(2)}) copy-start(bf16[128,2048]{1,0:T(8,128)(2,1)} %param.21) | copy-start | bytes 1572868
  57.6 24.1 %collective-permute-start.5 = (bf16[128,2048]{1,0:T(8,128)(2,1)S(1)}, bf16[128,2048]{1,0:T(8,128)(2,1)}, u32[]{:S(2)}, u32[]{:S(2)}) collective-permute-start(bf16[128,2048]{1,0:T(8,128)(2,1)S(1)} %collective-permute-done.3), channel_id=1, source_target_pairs={{0,15},{1,0},{2,1},{3,2},{4,3},{5,4},{6,5},{7,6},{8,7},{9,8},{10,9... | collective-permute-start | bytes 1572872 | tf_op jit(solution)/shard_map/ppermute | solution.py:24
  78.9 10.1 %collective-permute-start.6 = (bf16[128,2048]{1,0:T(8,128)(2,1)}, bf16[128,2048]{1,0:T(8,128)(2,1)}, u32[]{:S(2)}, u32[]{:S(2)}) collective-permute-start(bf16[128,2048]{1,0:T(8,128)(2,1)} %collective-permute-done.4), channel_id=1, source_target_pairs={{0,1},{1,2},{2,3},{3,4},{4,5},{5,6},{6,7},{7,8},{8,9},{9,10},{10,1... | collective-permute-start | bytes 1572872 | tf_op jit(solution)/shard_map/ppermute | solution.py:19
  81.7 9.9 %collective-permute-start.7 = (bf16[128,2048]{1,0:T(8,128)(2,1)}, bf16[128,2048]{1,0:T(8,128)(2,1)S(1)}, u32[]{:S(2)}, u32[]{:S(2)}) collective-permute-start(bf16[128,2048]{1,0:T(8,128)(2,1)} %collective-permute-done.5), channel_id=1, source_target_pairs={{0,15},{1,0},{2,1},{3,2},{4,3},{5,4},{6,5},{7,6},{8,7},{9,8},{10,9... | collective-permute-start | bytes 1572872 | tf_op jit(solution)/shard_map/ppermute | solution.py:24
  89.0 10.1 %collective-permute-start.8 = (bf16[128,2048]{1,0:T(8,128)(2,1)}, bf16[128,2048]{1,0:T(8,128)(2,1)}, u32[]{:S(2)}, u32[]{:S(2)}) collective-permute-start(bf16[128,2048]{1,0:T(8,128)(2,1)} %collective-permute-done.6), channel_id=1, source_target_pairs={{0,1},{1,2},{2,3},{3,4},{4,5},{5,6},{6,7},{7,8},{8,9},{9,10},{10,1... | collective-permute-start | bytes 1572872 | tf_op jit(solution)/shard_map/ppermute | solution.py:19
  91.6 9.7 %collective-permute-start.9 = (bf16[128,2048]{1,0:T(8,128)(2,1)S(1)}, bf16[128,2048]{1,0:T(8,128)(2,1)S(1)}, u32[]{:S(2)}, u32[]{:S(2)}) collective-permute-start(bf16[128,2048]{1,0:T(8,128)(2,1)S(1)} %collective-permute-done.7), channel_id=1, source_target_pairs={{0,15},{1,0},{2,1},{3,2},{4,3},{5,4},{6,5},{7,6},{8,7},{9,8},{10,9... | collective-permute-start | bytes 1572872 | tf_op jit(solution)/shard_map/ppermute | solution.py:24
  99.2 10.0 %collective-permute-start.10 = (bf16[128,2048]{1,0:T(8,128)(2,1)}, bf16[128,2048]{1,0:T(8,128)(2,1)S(1)}, u32[]{:S(2)}, u32[]{:S(2)}) collective-permute-start(bf16[128,2048]{1,0:T(8,128)(2,1)} %collective-permute-done.8), channel_id=1, source_target_pairs={{0,1},{1,2},{2,3},{3,4},{4,5},{5,6},{6,7},{7,8},{8,9},{9,10},{10,1... | collective-permute-start | bytes 1572872 | tf_op jit(solution)/shard_map/ppermute | solution.py:19
  101.3 10.6 %collective-permute-start.11 = (bf16[128,2048]{1,0:T(8,128)(2,1)S(1)}, bf16[128,2048]{1,0:T(8,128)(2,1)S(1)}, u32[]{:S(2)}, u32[]{:S(2)}) collective-permute-start(bf16[128,2048]{1,0:T(8,128)(2,1)S(1)} %collective-permute-done.9), channel_id=1, source_target_pairs={{0,15},{1,0},{2,1},{3,2},{4,3},{5,4},{6,5},{7,6},{8,7},{9,8},{10,9... | collective-permute-start | bytes 1572872 | tf_op jit(solution)/shard_map/ppermute | solution.py:24
  109.2 9.8 %collective-permute-start.12 = (bf16[128,2048]{1,0:T(8,128)(2,1)S(1)}, bf16[128,2048]{1,0:T(8,128)(2,1)S(1)}, u32[]{:S(2)}, u32[]{:S(2)}) collective-permute-start(bf16[128,2048]{1,0:T(8,128)(2,1)S(1)} %collective-permute-done.10), channel_id=1, source_target_pairs={{0,1},{1,2},{2,3},{3,4},{4,5},{5,6},{6,7},{7,8},{8,9},{9,10},{10,1... | collective-permute-start | bytes 1572872 | tf_op jit(solution)/shard_map/ppermute | solution.py:19
  111.9 9.7 %collective-permute-start.13 = (bf16[128,2048]{1,0:T(8,128)(2,1)S(1)}, bf16[128,2048]{1,0:T(8,128)(2,1)S(1)}, u32[]{:S(2)}, u32[]{:S(2)}) collective-permute-start(bf16[128,2048]{1,0:T(8,128)(2,1)S(1)} %collective-permute-done.11), channel_id=1, source_target_pairs={{0,15},{1,0},{2,1},{3,2},{4,3},{5,4},{6,5},{7,6},{8,7},{9,8},{10,9... | collective-permute-start | bytes 1572872 | tf_op jit(solution)/shard_map/ppermute | solution.py:24
  119.0 9.8 %collective-permute-start.14 = (bf16[128,2048]{1,0:T(8,128)(2,1)S(1)}, bf16[128,2048]{1,0:T(8,128)(2,1)S(1)}, u32[]{:S(2)}, u32[]{:S(2)}) collective-permute-start(bf16[128,2048]{1,0:T(8,128)(2,1)S(1)} %collective-permute-done.12), channel_id=1, source_target_pairs={{0,1},{1,2},{2,3},{3,4},{4,5},{5,6},{6,7},{7,8},{8,9},{9,10},{10,1... | collective-permute-start | bytes 1572872 | tf_op jit(solution)/shard_map/ppermute | solution.py:19
  121.6 9.8 %collective-permute-start.15 = (bf16[128,2048]{1,0:T(8,128)(2,1)S(1)}, bf16[128,2048]{1,0:T(8,128)(2,1)S(1)}, u32[]{:S(2)}, u32[]{:S(2)}) collective-permute-start(bf16[128,2048]{1,0:T(8,128)(2,1)S(1)} %collective-permute-done.13), channel_id=1, source_target_pairs={{0,15},{1,0},{2,1},{3,2},{4,3},{5,4},{6,5},{7,6},{8,7},{9,8},{10,9... | collective-permute-start | bytes 1572872 | tf_op jit(solution)/shard_map/ppermute | solution.py:24
  128.8 9.8 %collective-permute-start.16 = (bf16[128,2048]{1,0:T(8,128)(2,1)S(1)}, bf16[128,2048]{1,0:T(8,128)(2,1)S(1)}, u32[]{:S(2)}, u32[]{:S(2)}) collective-permute-start(bf16[128,2048]{1,0:T(8,128)(2,1)S(1)} %collective-permute-done.14), channel_id=1, source_target_pairs={{0,1},{1,2},{2,3},{3,4},{4,5},{5,6},{6,7},{7,8},{8,9},{9,10},{10,1... | collective-permute-start | bytes 1572872 | tf_op jit(solution)/shard_map/ppermute | solution.py:19
  129.7 9.8 %copy-start.14 = (bf16[192,2048]{1,0:T(8,128)(2,1)S(1)}, bf16[192,2048]{1,0:T(8,128)(2,1)}, u32[]{:S(2)}) copy-start(bf16[192,2048]{1,0:T(8,128)(2,1)} %param.22) | copy-start | bytes 2359300
  129.7 9.8 %copy-start.15 = (f32[2048]{0:T(1024)S(1)}, f32[2048]{0:T(1024)}, u32[]{:S(2)}) copy-start(f32[2048]{0:T(1024)} %param.20) | copy-start | bytes 24580
  129.7 9.8 %copy-start.16 = (f32[2048]{0:T(1024)S(1)}, f32[2048]{0:T(1024)}, u32[]{:S(2)}) copy-start(f32[2048]{0:T(1024)} %param.19) | copy-start | bytes 24580
  139.5 6.7 %copy-start.8 = (f32[2048]{0:T(1024)S(1)}, f32[2048]{0:T(1024)}, u32[]{:S(2)}) copy-start(f32[2048]{0:T(1024)} %param.23) | copy-start | bytes 24580
  145.1 1.2 copy-start.1
  149.6 23.6 %copy-start.13 = (bf16[1,2048,512]{2,1,0:T(8,128)(2,1)S(1)}, bf16[1,2048,512]{2,1,0:T(8,128)(2,1)}, u32[]{:S(2)}) copy-start(bf16[1,2048,512]{2,1,0:T(8,128)(2,1)} %param.27) | copy-start | bytes 6291460
  172.0 1.2 copy-start.3
  180.4 4.5 %copy-start.12 = (s32[384]{0:T(512)S(1)}, s32[384]{0:T(512)}, u32[]{:S(2)}) copy-start(s32[384]{0:T(512)} %copy-done.11) | copy-start | bytes 4612
  180.4 4.6 %copy-start.9 = (bf16[2048,2]{0,1:T(2,128)(2,1)S(1)}, bf16[2048,2]{0,1:T(2,128)(2,1)}, u32[]{:S(2)}) copy-start(bf16[2048,2]{0,1:T(2,128)(2,1)} %param.24) | copy-start | bytes 24580
  180.4 4.9 %copy-start.6 = (bf16[2048,16]{0,1:T(8,128)(2,1)S(1)}, bf16[2048,16]{0,1:T(8,128)(2,1)}, u32[]{:S(2)}) copy-start(bf16[2048,16]{0,1:T(8,128)(2,1)} %param.25) | copy-start | bytes 196612
  180.4 21.9 %all-to-all-start.2 = ((bf16[16,24,2048]{2,1,0:T(8,128)(2,1)}), bf16[16,24,2048]{2,1,0:T(8,128)(2,1)}, u32[]{:S(2)}, u32[]{:S(2)}) async-start(bf16[16,24,2048]{2,1,0:T(8,128)(2,1)} %bitcast.148), calls=%async_computation.2 | async-start | bytes 3145728 | tf_op jit(solution)/shard_map/all_to_all | solution.py:147
  213.6 6.2 %copy-start.2 = (f32[192,2048]{1,0:T(8,128)S(1)}, f32[192,2048]{1,0:T(8,128)}, u32[]{:S(2)}) copy-start(f32[192,2048]{1,0:T(8,128)} %copy-done.1) | copy-start | bytes 4718596
